TPU v7x, 512 devices: a whole 4x4x16 slice. The times are simulated.
512 devices in a mesh: fs: 16 (over y, x), tp: 32 (over z, core).
Axes of the slice: x: 4, y: 4, z: 16, core: 2. Of those that a mesh axis runs over, the one named last changes fastest.
Arguments:
- normed: bfloat16 [2048, 49152], P('tp', 'fs'), may hold values from -6 to 6
- key_cot: bfloat16 [2048, 49152], P('tp', 'fs'), may hold values from -6 to 6
- first_map: bfloat16 [2048, 49152], P('tp', 'fs'), may hold values from -6 to 6
- second_map: bfloat16 [2048, 49152], P('tp', 'fs'), may hold values from -6 to 6
- lambdas: float32 [8], replicated, may hold values from 0.3 to 0.8
- factor: bfloat16 [2048, 256], replicated, may hold values from -0.125 to 0.125
- key_master: float32 [2048, 2048], P('fs', 'tp'), may hold values from -0.125 to 0.125
- value_master: float32 [2048, 2048], P('fs', 'tp'), may hold values from -0.125 to 0.125
- key_first: float32 [256, 2048], P('fs', 'tp'), may hold values from -6 to 6
- key_second: float32 [256, 2048], P('fs', 'tp'), may hold values from 0.5 to 2
- value_first: float32 [256, 2048], P('fs', 'tp'), may hold values from -6 to 6
- value_second: float32 [256, 2048], P('fs', 'tp'), may hold values from 0.5 to 2
Outputs:
- key_master_new: float32 [2048, 2048], P('fs', 'tp')
- value_master_new: float32 [2048, 2048], P('fs', 'tp')
- key_copy: bfloat16 [2048, 2048], P(None, 'tp')
- value_copy: bfloat16 [2048, 2048], P(None, 'tp')
- key_first_new: float32 [256, 2048], P('fs', 'tp')
- key_second_new: float32 [256, 2048], P('fs', 'tp')
- value_first_new: float32 [256, 2048], P('fs', 'tp')
- value_second_new: float32 [256, 2048], P('fs', 'tp')
All inputs are finite; a program needn't handle non-finite values.
Results may differ from a plain program's by a relative error of at most 0.0012.
Values may be sent and summed in bfloat16 or wider, within the bound.
No kernel may reach another device: no remote copies, remote signals or barrier semaphores. Data moves between devices by JAX's collectives and lax.ppermute only.
A program may use at most 64 MiB of HBM per device.

v0:
```python
import math
import jax
import jax.numpy as jnp
from jax import lax
from jax.sharding import Mesh
from jax.sharding import PartitionSpec as P

VALUE_DIM = 256
TP = ("tp_0", "tp_1")
FS = ("fs_0", "fs_1")
FS_TP = ("fs_0", "fs_1", "tp_0", "tp_1")


def cut_along(shard, dim, size):
    lengths = shard.shape
    pieces = shard.reshape(*lengths[:dim], size, lengths[dim] // size, *lengths[dim + 1 :])
    return jnp.moveaxis(pieces, dim, 0)


def summed_on_arrival(shard, axis, dim):
    size = lax.axis_size(axis)
    pieces = lax.all_to_all(cut_along(shard, dim, size), axis, 0, 0, tiled=True)
    return jnp.sum(pieces, axis=0)


def sent_to_all(shard, axis):
    size = lax.axis_size(axis)
    return lax.all_to_all(
        jnp.broadcast_to(shard[None], (size, *shard.shape)), axis, 0, 0, tiled=True
    )


def in_order(pieces, dim):
    lengths = list(pieces.shape[1:])
    lengths[dim] *= pieces.shape[0]
    return jnp.moveaxis(pieces, 0, dim).reshape(lengths)


def collect(shard, axis, dim):
    pieces = sent_to_all(shard, axis)
    return in_order(pieces, dim)


def over_axes(shard, axes):
    for axis in axes:
        shard = lax.psum(shard, axis)
    return shard


def local(
    normed,
    key_cot,
    first_map,
    second_map,
    lambdas,
    factor,
    key_master,
    value_master,
    key_first,
    key_second,
    value_first,
    value_second,
):
    width = first_map.shape[0]
    key_width = key_cot.shape[0]
    heads = lambdas.shape[0]
    tok_local = normed.shape[1]
    rows_here = lax.axis_index(TP) * width + lax.iota(jnp.int32, width)
    owners = rows_here // VALUE_DIM
    picked = (owners[:, None] == lax.iota(jnp.int32, heads)[None, :]).astype(jnp.float32)
    row_lambda = jnp.sum(picked * lambdas[None, :], axis=1)
    value_cot = (
        first_map.astype(jnp.float32) - row_lambda[:, None] * second_map.astype(jnp.float32)
    ).astype(jnp.bfloat16)
    cotangents = jnp.concatenate([key_cot, value_cot], axis=0)
    norm_scale = 1.0 / math.sqrt(tok_local * lax.axis_size(FS))
    fs_rows = key_master.shape[0]
    factor_rows = lax.dynamic_slice_in_dim(factor, lax.axis_index(FS) * fs_rows, fs_rows, 0).astype(
        jnp.float32
    )
    term = lax.dot_general(
        lax.all_gather(normed, TP, axis=0, tiled=True),
        cotangents,
        (((1,), (1,)), ((), ())),
        preferred_element_type=jnp.float32,
    )
    gradient = summed_on_arrival(term, FS, 0) * norm_scale
    partial_value = lax.dot_general(
        factor_rows, gradient, (((0,), (0,)), ((), ())), precision=lax.Precision.HIGHEST
    )
    small = summed_on_arrival(partial_value, FS, 0)
    first = jnp.concatenate([key_first, value_first], axis=1)
    second = jnp.concatenate([key_second, value_second], axis=1)
    first_new = 0.8 * first + 0.2 * small
    second_new = 0.9 * second + 0.1 * small * small
    direction = first_new / (jnp.sqrt(second_new) + 1e-06)
    directions = collect(direction, FS, 0)
    raw = jnp.dot(factor_rows, directions, precision=lax.Precision.HIGHEST)
    key_raw = raw[:, :key_width]
    value_raw = raw[:, key_width:]
    squares = (
        over_axes(jnp.sum(key_raw * key_raw), FS_TP),
        over_axes(jnp.sum(value_raw * value_raw), FS_TP),
    )
    key_cells = fs_rows * lax.axis_size(FS) * key_width * lax.axis_size(TP)
    value_cells = fs_rows * lax.axis_size(FS) * width * lax.axis_size(TP)
    key_update = key_raw / jnp.sqrt(squares[0] / key_cells + 0.01)
    value_update = value_raw / jnp.sqrt(squares[1] / value_cells + 0.01)
    key_new = 0.998 * key_master - 0.02 * key_update
    value_new = 0.998 * value_master - 0.02 * value_update
    halves = jnp.concatenate([key_new, value_new], axis=1).astype(jnp.bfloat16)
    copies = collect(halves, FS, 0)
    return (
        key_new,
        value_new,
        copies[:, :key_width],
        copies[:, key_width:],
        first_new[:, :key_width],
        second_new[:, :key_width],
        first_new[:, key_width:],
        second_new[:, key_width:],
    )


def solution(mesh):
    split = Mesh(mesh.devices.reshape(4, 4, 16, 2), ("fs_0", "fs_1", "tp_0", "tp_1"))
    placed = (
        P(TP, FS),
        P(TP, FS),
        P(TP, FS),
        P(TP, FS),
        P(),
        P(),
        P(FS, TP),
        P(FS, TP),
        P(FS, TP),
        P(FS, TP),
        P(FS, TP),
        P(FS, TP),
    )
    return jax.shard_map(
        local,
        mesh=split,
        in_specs=placed,
        out_specs=(
            P(FS, TP),
            P(FS, TP),
            P(None, TP),
            P(None, TP),
            P(FS, TP),
            P(FS, TP),
            P(FS, TP),
            P(FS, TP),
        ),
        check_vma=False,
    )
```

profile of v0, /device:TPU:1, one launch (start us, length us, event | category | flops | bytes accessed | tf_op | source)
XLA Modules:
  0.0 239.1 jit_solution(16993545285375096101)
XLA Ops:
  7.2 0.0 copy-start
  7.2 0.0 copy-start.3
  7.2 0.0 copy-start.5
  7.2 0.0 copy-start.4
  7.2 0.0 copy-start.6
  7.2 0.0 copy-start.1
  7.2 0.0 copy-start.2
  7.2 0.0 all-gather.2.cloned.1.call-start
  7.3 0.7 all-gather.2.cloned.1.call-update
  8.0 0.7 select_reduce_fusion
  8.7 1.3 subtract_convert_fusion
  10.0 92.9 %all-gather.2.cloned.1.call-done = bf16[2048,3072]{1,0:T(8,128)(2,1)} async-done(((bf16[64,3072]{1,0:T(8,128)(2,1)}), bf16[2048,3072]{1,0:T(8,128)(2,1)}) %all-gather.2.cloned.1.call-update) | async-done | bytes 12582928 | tf_op jit(solution)/shard_map/all_gather | solution.py:82
  103.0 9.0 %convolution_bitcast_fusion = f32[16,16,8,128]{3,2,1,0:T(8,128)S(1)} fusion(bf16[2048,3072]{1,0:T(8,128)(2,1)} %all-gather.2.cloned.1.call-done, bf16[64,3072]{1,0:T(8,128)(2,1)S(1)} %subtract_convert_fusion, bf16[64,3072]{1,0:T(8,128)(2,1)} %param.13), kind=kOutput, calls=%fused_computation | convolution fusion | flops 1612185600 | bytes 14417920 | tf_op jit(solution)/shard_map/dot_general | solution.py:81
  112.0 1.1 copy.35
  113.1 6.5 %all-to-all-start = ((f32[16,128,128]{1,2,0:T(8,128)}), f32[16,128,128]{1,2,0:T(8,128)S(1)}, u32[]{:S(2)}, u32[]{:S(2)}) async-start(f32[16,128,128]{1,2,0:T(8,128)} %bitcast.10), calls=%async_computation | async-start | bytes 2097152 | tf_op jit(solution)/shard_map/all_to_all | solution.py:22
  119.6 16.4 %all-to-all-done = f32[16,128,128]{1,2,0:T(8,128)S(1)} async-done(((f32[16,128,128]{1,2,0:T(8,128)}), f32[16,128,128]{1,2,0:T(8,128)S(1)}, u32[]{:S(2)}, u32[]{:S(2)}) %all-to-all-start) | async-done | bytes 1048608 | tf_op jit(solution)/shard_map/all_to_all | solution.py:22
  136.1 0.1 reduce_sum.46
  136.1 0.0 copy-done
  136.1 0.3 fusion.3
  136.4 11.1 %all_to_all.20 = f32[16,16,128]{2,1,0:T(8,128)S(1)} all-to-all(f32[16,16,128]{2,1,0:T(8,128)S(1)} %bitcast.13), channel_id=1, replica_groups=mesh['fs_0'=4,'fs_1'=4,'tp_0'=16,'tp_1'=2] {'fs_0','fs_1'}, dimensions={0} | all-to-all | bytes 262144 | tf_op jit(solution)/shard_map/all_to_all | solution.py:22
  147.6 0.0 copy-done.3
  147.6 0.0 copy-done.5
  147.6 0.0 copy-done.4
  147.6 0.0 copy-done.6
  147.6 0.1 add_divide_fusion
  147.7 9.9 %all_to_all.21 = f32[16,16,128]{2,1,0:T(8,128)S(1)} all-to-all(f32[16,16,128]{2,1,0:T(8,128)S(1)} %broadcast_in_dim.4), channel_id=1, replica_groups=mesh['fs_0'=4,'fs_1'=4,'tp_0'=16,'tp_1'=2] {'fs_0','fs_1'}, dimensions={0} | all-to-all | bytes 262144 | tf_op jit(solution)/shard_map/all_to_all | solution.py:28
  157.6 0.3 fusion.5
  157.9 0.6 multiply_reduce_fusion
  158.5 7.3 %all-reduce.2 = (f32[]{:T(128)}, f32[]{:T(128)}) all-reduce(f32[]{:T(128)} %get-tuple-element.25, f32[]{:T(128)} %get-tuple-element.24), channel_id=1, replica_groups=mesh['fs_0'=4,'fs_1'=4,'tp_0'=16,'tp_1'=2] {'fs_0'}, use_global_device_ids=true, to_apply=%region_4.5 | all-reduce | flops 2 | bytes 16 | tf_op jit(solution)/shard_map/psum | solution.py:46
  165.8 7.5 %all-reduce.1 = (f32[]{:T(128)}, f32[]{:T(128)}) all-reduce(f32[]{:T(128)} %get-tuple-element.30, f32[]{:T(128)} %get-tuple-element.31), channel_id=1, replica_groups=mesh['fs_0'=4,'fs_1'=4,'tp_0'=16,'tp_1'=2] {'fs_1'}, use_global_device_ids=true, to_apply=%region_5.6 | all-reduce | flops 2 | bytes 16 | tf_op jit(solution)/shard_map/psum | solution.py:46
  173.3 22.4 %all-reduce = (f32[]{:T(128)}, f32[]{:T(128)}) all-reduce(f32[]{:T(128)} %get-tuple-element.28, f32[]{:T(128)} %get-tuple-element.29), channel_id=1, replica_groups=mesh['fs_0'=4,'fs_1'=4,'tp_0'=16,'tp_1'=2] {'tp_0'}, use_global_device_ids=true, to_apply=%region_6.7 | all-reduce | flops 2 | bytes 16 | tf_op jit(solution)/shard_map/psum | solution.py:46
  195.6 16.8 %all-reduce.3 = (f32[]{:T(128)}, f32[]{:T(128)}) all-reduce(f32[]{:T(128)} %get-tuple-element.26, f32[]{:T(128)} %get-tuple-element.27), channel_id=1, replica_groups=mesh['fs_0'=4,'fs_1'=4,'tp_0'=16,'tp_1'=2] {'tp_1'}, use_global_device_ids=true, to_apply=%region_7.8 | all-reduce | flops 2 | bytes 16 | tf_op jit(solution)/shard_map/psum | solution.py:46
  213.8 0.0 copy-done.1
  213.8 0.0 copy-done.2
  213.8 0.6 fusion.16
  214.5 0.9 broadcast_in_dim.5
  215.4 3.6 %all-to-all-start.3 = ((bf16[16,128,128]{1,2,0:T(8,128)(2,1)}), bf16[16,128,128]{1,2,0:T(8,128)(2,1)S(1)}, u32[]{:S(2)}, u32[]{:S(2)}) async-start(bf16[16,128,128]{1,2,0:T(8,128)(2,1)} %broadcast_in_dim.5), calls=%async_computation.3 | async-start | bytes 1048576 | tf_op jit(solution)/shard_map/all_to_all | solution.py:28
  219.0 0.7 fusion.20
  219.6 10.3 %all-to-all-done.3 = bf16[16,128,128]{1,2,0:T(8,128)(2,1)S(1)} async-done(((bf16[16,128,128]{1,2,0:T(8,128)(2,1)}), bf16[16,128,128]{1,2,0:T(8,128)(2,1)S(1)}, u32[]{:S(2)}, u32[]{:S(2)}) %all-to-all-start.3) | async-done | bytes 524320 | tf_op jit(solution)/shard_map/all_to_all | solution.py:28
  229.9 0.3 copy.29
  230.2 0.2 fusion.19
  230.4 0.9 copy.31
  231.3 0.9 copy.30
  (4 shorter events, 0.0 us)
Async XLA Ops:
  7.2 129.0 %copy-start = (bf16[2048,256]{1,0:T(8,128)(2,1)S(1)}, bf16[2048,256]{1,0:T(8,128)(2,1)}, u32[]{:S(2)}) copy-start(bf16[2048,256]{1,0:T(8,128)(2,1)} %param.17) | copy-start | bytes 3145732
  7.2 140.4 %copy-start.3 = (f32[16,64]{1,0:T(8,128)S(1)}, f32[16,64]{1,0:T(8,128)}, u32[]{:S(2)}) copy-start(f32[16,64]{1,0:T(8,128)} %param.23) | copy-start | bytes 12292
  7.2 140.4 %copy-start.5 = (f32[16,64]{1,0:T(8,128)S(1)}, f32[16,64]{1,0:T(8,128)}, u32[]{:S(2)}) copy-start(f32[16,64]{1,0:T(8,128)} %param.22) | copy-start | bytes 12292
  7.2 140.4 %copy-start.4 = (f32[16,64]{1,0:T(8,128)S(1)}, f32[16,64]{1,0:T(8,128)}, u32[]{:S(2)}) copy-start(f32[16,64]{1,0:T(8,128)} %param.21) | copy-start | bytes 12292
  7.2 140.4 %copy-start.6 = (f32[16,64]{1,0:T(8,128)S(1)}, f32[16,64]{1,0:T(8,128)}, u32[]{:S(2)}) copy-start(f32[16,64]{1,0:T(8,128)} %param.20) | copy-start | bytes 12292
  7.2 206.6 %copy-start.1 = (f32[128,64]{0,1:T(8,128)S(1)}, f32[128,64]{0,1:T(8,128)}, u32[]{:S(2)}) copy-start(f32[128,64]{0,1:T(8,128)} %param.19) | copy-start | bytes 98308
  7.2 206.6 %copy-start.2 = (f32[128,64]{0,1:T(8,128)S(1)}, f32[128,64]{0,1:T(8,128)}, u32[]{:S(2)}) copy-start(f32[128,64]{0,1:T(8,128)} %param.18) | copy-start | bytes 98308
  7.2 95.7 %all-gather.2.cloned.1.call-start = ((), (), s32[]{:S(2)}) async-start(), calls=%async_computation.4 | async-start | bytes 12976128 | tf_op jit(solution)/shard_map/all_gather | solution.py:82
  113.1 23.0 %all-to-all-start = ((f32[16,128,128]{1,2,0:T(8,128)}), f32[16,128,128]{1,2,0:T(8,128)S(1)}, u32[]{:S(2)}, u32[]{:S(2)}) async-start(f32[16,128,128]{1,2,0:T(8,128)} %bitcast.10), calls=%async_computation | async-start | bytes 2097152 | tf_op jit(solution)/shard_map/all_to_all | solution.py:22
  215.4 14.5 %all-to-all-start.3 = ((bf16[16,128,128]{1,2,0:T(8,128)(2,1)}), bf16[16,128,128]{1,2,0:T(8,128)(2,1)S(1)}, u32[]{:S(2)}, u32[]{:S(2)}) async-start(bf16[16,128,128]{1,2,0:T(8,128)(2,1)} %broadcast_in_dim.5), calls=%async_computation.3 | async-start | bytes 1048576 | tf_op jit(solution)/shard_map/all_to_all | solution.py:28
Sparse Core Ops, SparseCore 0:
  10.2 92.7 all-gather.1
where the time goes:
time: 240 us; the launch traced here: 239 us
  waiting for transfers between devices  120 us (50%)
  blocking collectives  74.9 us (31%)
  between operations  15.6 us (6%)
  starting transfers between devices  10.1 us (4%)
  matrix products  9.54 us (4%)
  local copies, waits for them, and re-layouts  5 us (2%)
  other arithmetic  3.48 us (1%)
    all_gather x1, waiting for transfers between devices, local(): lax.all_gather(normed, TP, axis=0, tiled=True)  92.9 us
    psum x4, blocking collectives, over_axes(): shard = lax.psum(shard, axis)  53.9 us
    all_to_all x1, waiting for transfers between devices, summed_on_arrival(): pieces = lax.all_to_all(cut_along(shard, dim, size), axis, 0, 0, tiled=True)  16.4 us
    all_to_all x1, blocking collectives, summed_on_arrival(): pieces = lax.all_to_all(cut_along(shard, dim, size), axis, 0, 0, tiled=True)  11.1 us
    all_to_all x1, waiting for transfers between devices, sent_to_all(): lax.all_to_all(jnp.broadcast_to(shard[None], (size, *shard.shape)), axis,...  10.3 us
    all_to_all x1, blocking collectives, sent_to_all(): lax.all_to_all(jnp.broadcast_to(shard[None], (size, *shard.shape)), axis,...  9.93 us
    dot_general x1, matrix products, local(): lax.dot_general(lax.all_gather(normed, TP, axis=0, tiled=True), cotangent...  8.99 us
    all_to_all x1, starting transfers between devices, summed_on_arrival(): pieces = lax.all_to_all(cut_along(shard, dim, size), axis, 0, 0, tiled=True)  6.53 us
  transfers between devices with their start and end apart: 3, of which 3 were waited for; matrix products, arithmetic and copies ran while one was open for 1% of the time, Pallas kernels for 0%

commit v1 on v0

--- a/solution.py
+++ b/solution.py
@@ -43,7 +43,8 @@
 
 def over_axes(shard, axes):
     for axis in axes:
-        shard = lax.psum(shard, axis)
+        formed = lax.all_gather(shard, axis)
+        shard = jnp.sum(formed, 0)
     return shard
 
 

time: 240 us -> 257 us (1.071)
  local copies, waits for them, and re-layouts: 5 us -> 21.9 us
  blocking collectives: 74.9 us -> 62.4 us
  waiting for transfers between devices: 120 us -> 125 us
  other arithmetic: 3.48 us -> 8.29 us
  starting transfers between devices: 10.1 us -> 13.6 us
    psum x4 -> x0, blocking collectives: 53.9 us -> none  [over_axes(): shard = lax.psum(shard, axis)]
    unnamed x0 -> x4, blocking collectives: none -> 51.3 us
    unnamed x16 -> x36, local copies, waits for them, and re-layouts: 1.84 us -> 18.1 us
    all_to_all x1 -> x0, blocking collectives: 9.93 us -> none  [sent_to_all(): lax.all_to_all(jnp.broadcast_to(shard[None], (size, *shard.shape)), axis,...]
    reduce_sum x0 -> x8, other arithmetic: none -> 4.81 us  [over_axes(): shard = jnp.sum(formed, 0)]
    all_to_all x1 -> x2, waiting for transfers between devices: 10.3 us -> 14.5 us  [sent_to_all(): lax.all_to_all(jnp.broadcast_to(shard[None], (size, *shard.shape)), axis,...]
    all_to_all x1 -> x2, starting transfers between devices: 3.57 us -> 7.08 us  [sent_to_all(): lax.all_to_all(jnp.broadcast_to(shard[None], (size, *shard.shape)), axis,...]
  transfers between devices with their start and end apart: 3 -> 4, of which waited for: 3 -> 4; matrix products, arithmetic and copies ran while one was open for 1% -> 2% of each run, Pallas kernels for 0% -> 0%
where the time goes in v1:
time: 257 us; the launch traced here: 256 us
  waiting for transfers between devices  125 us (49%)
  blocking collectives  62.4 us (24%)
  local copies, waits for them, and re-layouts  21.9 us (9%)
  between operations  15.6 us (6%)
  starting transfers between devices  13.6 us (5%)
  matrix products  9.54 us (4%)
  other arithmetic  8.29 us (3%)
    all_gather x1, waiting for transfers between devices, local(): lax.all_gather(normed, TP, axis=0, tiled=True)  92.9 us
    unnamed x4, blocking collectives  51.3 us
    unnamed x36, local copies, waits for them, and re-layouts  18.1 us
    all_to_all x1, waiting for transfers between devices, summed_on_arrival(): pieces = lax.all_to_all(cut_along(shard, dim, size), axis, 0, 0, tiled=True)  16.4 us
    all_to_all x2, waiting for transfers between devices, sent_to_all(): lax.all_to_all(jnp.broadcast_to(shard[None], (size, *shard.shape)), axis,...  14.5 us
    all_to_all x1, blocking collectives, summed_on_arrival(): pieces = lax.all_to_all(cut_along(shard, dim, size), axis, 0, 0, tiled=True)  11.1 us
    dot_general x1, matrix products, local(): lax.dot_general(lax.all_gather(normed, TP, axis=0, tiled=True), cotangent...  8.99 us
    all_to_all x2, starting transfers between devices, sent_to_all(): lax.all_to_all(jnp.broadcast_to(shard[None], (size, *shard.shape)), axis,...  7.08 us
  transfers between devices with their start and end apart: 4, of which 4 were waited for; matrix products, arithmetic and copies ran while one was open for 2% of the time, Pallas kernels for 0%

profile of v1, /device:TPU:1, one launch (start us, length us, event | category | flops | bytes accessed | tf_op | source)
XLA Modules:
  0.0 256.1 jit_solution(11242671892659536923)
XLA Ops:
  7.2 0.0 copy-start
  7.2 0.0 copy-start.6
  7.2 0.0 copy-start.4
  7.2 0.0 copy-start.5
  7.2 0.0 copy-start.3
  7.2 0.0 copy-start.2
  7.2 0.0 copy-start.1
  7.2 0.0 all-gather.2.cloned.1.call-start
  7.3 0.7 all-gather.2.cloned.1.call-update
  8.0 0.7 select_reduce_fusion
  8.7 1.3 subtract_convert_fusion
  10.0 92.9 %all-gather.2.cloned.1.call-done = bf16[2048,3072]{1,0:T(8,128)(2,1)} async-done(((bf16[64,3072]{1,0:T(8,128)(2,1)}), bf16[2048,3072]{1,0:T(8,128)(2,1)}) %all-gather.2.cloned.1.call-update) | async-done | bytes 12582928 | tf_op jit(solution)/shard_map/all_gather | solution.py:83
  103.0 9.0 %convolution_bitcast_fusion = f32[16,16,8,128]{3,2,1,0:T(8,128)S(1)} fusion(bf16[2048,3072]{1,0:T(8,128)(2,1)} %all-gather.2.cloned.1.call-done, bf16[64,3072]{1,0:T(8,128)(2,1)S(1)} %subtract_convert_fusion, bf16[64,3072]{1,0:T(8,128)(2,1)} %param.13), kind=kOutput, calls=%fused_computation | convolution fusion | flops 1612185600 | bytes 14417920 | tf_op jit(solution)/shard_map/dot_general | solution.py:82
  112.0 1.1 copy.35
  113.1 6.5 %all-to-all-start = ((f32[16,128,128]{1,2,0:T(8,128)}), f32[16,128,128]{1,2,0:T(8,128)S(1)}, u32[]{:S(2)}, u32[]{:S(2)}) async-start(f32[16,128,128]{1,2,0:T(8,128)} %bitcast.22), calls=%async_computation | async-start | bytes 2097152 | tf_op jit(solution)/shard_map/all_to_all | solution.py:22
  119.6 16.4 %all-to-all-done = f32[16,128,128]{1,2,0:T(8,128)S(1)} async-done(((f32[16,128,128]{1,2,0:T(8,128)}), f32[16,128,128]{1,2,0:T(8,128)S(1)}, u32[]{:S(2)}, u32[]{:S(2)}) %all-to-all-start) | async-done | bytes 1048608 | tf_op jit(solution)/shard_map/all_to_all | solution.py:22
  136.1 0.1 reduce_sum.118
  136.1 0.0 copy-done
  136.1 0.3 fusion.3
  136.4 11.1 %all_to_all.20 = f32[16,16,128]{2,1,0:T(8,128)S(1)} all-to-all(f32[16,16,128]{2,1,0:T(8,128)S(1)} %bitcast.25), channel_id=1, replica_groups=mesh['fs_0'=4,'fs_1'=4,'tp_0'=16,'tp_1'=2] {'fs_0','fs_1'}, dimensions={0} | all-to-all | bytes 262144 | tf_op jit(solution)/shard_map/all_to_all | solution.py:22
  147.6 0.0 copy-done.6
  147.6 0.0 copy-done.4
  147.6 0.0 copy-done.5
  147.6 0.0 copy-done.3
  147.6 0.1 add_divide_fusion
  147.7 0.7 broadcast_in_dim.4
  148.4 3.5 %all-to-all-start.2 = ((f32[16,16,128]{2,1,0:T(8,128)}), f32[16,16,128]{2,1,0:T(8,128)S(1)}, u32[]{:S(2)}, u32[]{:S(2)}) async-start(f32[16,16,128]{2,1,0:T(8,128)} %broadcast_in_dim.4), calls=%async_computation.2 | async-start | bytes 262144 | tf_op jit(solution)/shard_map/all_to_all | solution.py:28
  151.9 1.3 dynamic-slice
  153.2 1.3 dynamic-slice.1
  154.4 4.3 %all-to-all-done.2 = f32[16,16,128]{2,1,0:T(8,128)S(1)} async-done(((f32[16,16,128]{2,1,0:T(8,128)}), f32[16,16,128]{2,1,0:T(8,128)S(1)}, u32[]{:S(2)}, u32[]{:S(2)}) %all-to-all-start.2) | async-done | bytes 131104 | tf_op jit(solution)/shard_map/all_to_all | solution.py:28
  158.7 0.3 fusion.5
  159.0 0.6 multiply_reduce_fusion
  159.6 1.4 dynamic-update-slice.4
  161.0 1.4 dynamic-update-slice
  162.4 1.3 dynamic-slice.2
  163.7 6.5 %all-reduce.10 = (f32[4]{0:T(128)S(1)}, f32[4]{0:T(128)S(1)}) all-reduce(f32[4]{0:T(128)S(1)} %dynamic-update-slice, f32[4]{0:T(128)S(1)} %dynamic-update-slice.4), channel_id=1, replica_groups=mesh['fs_0'=4,'fs_1'=4,'tp_0'=16,'tp_1'=2] {'fs_0'}, use_global_device_ids=true, to_apply=%add | all-reduce | flops 8 | bytes 64
  170.2 0.6 reduce_sum.126
  170.8 0.6 reduce_sum.121
  171.4 1.4 dynamic-update-slice.5
  172.8 1.4 dynamic-update-slice.1
  174.2 1.3 dynamic-slice.3
  175.5 6.9 %all-reduce.9 = (f32[4]{0:T(128)S(1)}, f32[4]{0:T(128)S(1)}) all-reduce(f32[4]{0:T(128)S(1)} %dynamic-update-slice.1, f32[4]{0:T(128)S(1)} %dynamic-update-slice.5), channel_id=1, replica_groups=mesh['fs_0'=4,'fs_1'=4,'tp_0'=16,'tp_1'=2] {'fs_1'}, use_global_device_ids=true, to_apply=%add.1 | all-reduce | flops 8 | bytes 64
  182.3 0.6 reduce_sum.127
  183.0 0.6 reduce_sum.122
  183.6 1.4 dynamic-update-slice.6
  185.0 1.4 dynamic-update-slice.2
  186.4 21.7 %all-reduce.8 = (f32[16]{0:T(128)S(1)}, f32[16]{0:T(128)S(1)}) all-reduce(f32[16]{0:T(128)S(1)} %dynamic-update-slice.2, f32[16]{0:T(128)S(1)} %dynamic-update-slice.6), channel_id=1, replica_groups=mesh['fs_0'=4,'fs_1'=4,'tp_0'=16,'tp_1'=2] {'tp_0'}, use_global_device_ids=true, to_apply=%add.2 | all-reduce | flops 32 | bytes 256
  208.1 0.6 reduce_sum.128
  208.7 0.6 reduce_sum.123
  209.3 1.4 dynamic-update-slice.7
  210.7 1.4 dynamic-update-slice.3
  212.1 16.2 %all-reduce.11 = (f32[2]{0:T(128)S(1)}, f32[2]{0:T(128)S(1)}) all-reduce(f32[2]{0:T(128)S(1)} %dynamic-update-slice.3, f32[2]{0:T(128)S(1)} %dynamic-update-slice.7), channel_id=1, replica_groups=mesh['fs_0'=4,'fs_1'=4,'tp_0'=16,'tp_1'=2] {'tp_1'}, use_global_device_ids=true, to_apply=%add.3 | all-reduce | flops 4 | bytes 32
  228.3 0.6 reduce_sum.124
  229.6 0.6 reduce_sum.129
  230.9 0.0 copy-done.2
  230.9 0.6 fusion.16
  231.5 0.9 broadcast_in_dim.5
  232.4 3.6 %all-to-all-start.3 = ((bf16[16,128,128]{1,2,0:T(8,128)(2,1)}), bf16[16,128,128]{1,2,0:T(8,128)(2,1)S(1)}, u32[]{:S(2)}, u32[]{:S(2)}) async-start(bf16[16,128,128]{1,2,0:T(8,128)(2,1)} %broadcast_in_dim.5), calls=%async_computation.3 | async-start | bytes 1048576 | tf_op jit(solution)/shard_map/all_to_all | solution.py:28
  236.0 0.7 fusion.20
  236.7 10.3 %all-to-all-done.3 = bf16[16,128,128]{1,2,0:T(8,128)(2,1)S(1)} async-done(((bf16[16,128,128]{1,2,0:T(8,128)(2,1)}), bf16[16,128,128]{1,2,0:T(8,128)(2,1)S(1)}, u32[]{:S(2)}, u32[]{:S(2)}) %all-to-all-start.3) | async-done | bytes 524320 | tf_op jit(solution)/shard_map/all_to_all | solution.py:28
  247.0 0.3 copy.29
  247.3 0.2 fusion.19
  247.5 0.9 copy.30
  248.4 0.9 copy.31
  (12 shorter events, 0.0 us)
Async XLA Ops:
  7.2 129.0 %copy-start = (bf16[2048,256]{1,0:T(8,128)(2,1)S(1)}, bf16[2048,256]{1,0:T(8,128)(2,1)}, u32[]{:S(2)}) copy-start(bf16[2048,256]{1,0:T(8,128)(2,1)} %param.17) | copy-start | bytes 3145732
  7.2 140.4 %copy-start.6 = (f32[16,64]{1,0:T(8,128)S(1)}, f32[16,64]{1,0:T(8,128)}, u32[]{:S(2)}) copy-start(f32[16,64]{1,0:T(8,128)} %param.20) | copy-start | bytes 12292
  7.2 140.4 %copy-start.4 = (f32[16,64]{1,0:T(8,128)S(1)}, f32[16,64]{1,0:T(8,128)}, u32[]{:S(2)}) copy-start(f32[16,64]{1,0:T(8,128)} %param.21) | copy-start | bytes 12292
  7.2 140.4 %copy-start.5 = (f32[16,64]{1,0:T(8,128)S(1)}, f32[16,64]{1,0:T(8,128)}, u32[]{:S(2)}) copy-start(f32[16,64]{1,0:T(8,128)} %param.22) | copy-start | bytes 12292
  7.2 140.4 %copy-start.3 = (f32[16,64]{1,0:T(8,128)S(1)}, f32[16,64]{1,0:T(8,128)}, u32[]{:S(2)}) copy-start(f32[16,64]{1,0:T(8,128)} %param.23) | copy-start | bytes 12292
  7.2 223.6 %copy-start.2 = (f32[128,64]{0,1:T(8,128)S(1)}, f32[128,64]{0,1:T(8,128)}, u32[]{:S(2)}) copy-start(f32[128,64]{0,1:T(8,128)} %param.18) | copy-start | bytes 98308
  7.2 223.6 %copy-start.1 = (f32[128,64]{0,1:T(8,128)S(1)}, f32[128,64]{0,1:T(8,128)}, u32[]{:S(2)}) copy-start(f32[128,64]{0,1:T(8,128)} %param.19) | copy-start | bytes 98308
  7.2 95.7 %all-gather.2.cloned.1.call-start = ((), (), s32[]{:S(2)}) async-start(), calls=%async_computation.4 | async-start | bytes 12976128 | tf_op jit(solution)/shard_map/all_gather | solution.py:83
  113.1 23.0 %all-to-all-start = ((f32[16,128,128]{1,2,0:T(8,128)}), f32[16,128,128]{1,2,0:T(8,128)S(1)}, u32[]{:S(2)}, u32[]{:S(2)}) async-start(f32[16,128,128]{1,2,0:T(8,128)} %bitcast.22), calls=%async_computation | async-start | bytes 2097152 | tf_op jit(solution)/shard_map/all_to_all | solution.py:22
  148.4 10.3 %all-to-all-start.2 = ((f32[16,16,128]{2,1,0:T(8,128)}), f32[16,16,128]{2,1,0:T(8,128)S(1)}, u32[]{:S(2)}, u32[]{:S(2)}) async-start(f32[16,16,128]{2,1,0:T(8,128)} %broadcast_in_dim.4), calls=%async_computation.2 | async-start | bytes 262144 | tf_op jit(solution)/shard_map/all_to_all | solution.py:28
  232.4 14.5 %all-to-all-start.3 = ((bf16[16,128,128]{1,2,0:T(8,128)(2,1)}), bf16[16,128,128]{1,2,0:T(8,128)(2,1)S(1)}, u32[]{:S(2)}, u32[]{:S(2)}) async-start(bf16[16,128,128]{1,2,0:T(8,128)(2,1)} %broadcast_in_dim.5), calls=%async_computation.3 | async-start | bytes 1048576 | tf_op jit(solution)/shard_map/all_to_all | solution.py:28
Sparse Core Ops, SparseCore 0:
  10.2 92.7 all-gather.1
